TPU v7x, 32 devices: a whole 2x2x4 slice. The times are simulated.
32 devices in a mesh: sp: 8 (over z, y), tp: 4 (over x, core).
Axes of the slice: x: 2, y: 2, z: 4, core: 2. Of those that a mesh axis runs over, the one named last changes fastest.
Arguments:
- inputs: bfloat16 [2, 1024, 2048], P(None, 'sp'), may hold values from -6 to 6
- norm_gain: float32 [2048], replicated, may hold values from 0.1 to 1.9
- query_weight: bfloat16 [2048, 1024], P('sp', 'tp'), may hold values from -0.125 to 0.125
- key_weight: bfloat16 [2048, 256], P('sp', 'tp'), may hold values from -0.125 to 0.125
- value_weight: bfloat16 [2048, 256], P('sp', 'tp'), may hold values from -0.125 to 0.125
- query_gain: float32 [64], replicated, may hold values from 0.1 to 24
- key_gain: float32 [64], replicated, may hold values from 0.1 to 1.9
- forget_cache: float32 [2, 16, 1024], P(None, 'tp'), may hold values from -104 to 0, as said below
- rec_in_weight: bfloat16 [2048, 1024], P('sp', 'tp'), may hold values from -0.125 to 0.125
- rec_gate_weight: bfloat16 [2048, 1024], P('sp', 'tp'), may hold values from -0.125 to 0.125
- conv_weight: bfloat16 [4, 1024], P(None, 'tp'), may hold values from -3 to 3
- decay_gate_weight: bfloat16 [16, 64, 64], P('tp'), may hold values from -0.75 to 0.75
- input_gate_weight: bfloat16 [16, 64, 64], P('tp'), may hold values from -0.75 to 0.75
- decay_param: float32 [1024], P('tp'), may hold values from 4 to 16
- decay_extra: float32 [2, 1024, 1024], P(None, 'sp', 'tp'), may hold values from -2 to 0
- attn_out_gain: float32 [1024], P('tp'), may hold values from 0.1 to 1.9
- rec_out_gain: float32 [1024], P('tp'), may hold values from 0.1 to 1.9
- out_att_weight: bfloat16 [1024, 2048], P('tp'), may hold values from -0.125 to 0.125
- out_rec_weight: bfloat16 [1024, 2048], P('tp'), may hold values from -0.125 to 0.125
Outputs:
- mixed: bfloat16 [2, 1024, 2048], P(None, 'sp', 'tp')
Inputs may be any that keep to these rules, and one draw needn't show every extreme that they name: `forget_cache`: Non-increasing along the positions of each sequence and head.
All inputs are finite; a program needn't handle non-finite values.
Results may differ from a plain program's by a relative error of at most 0.012.
The roundings to bfloat16 on the way count: a program that leaves them out, or rounds other values in their place, can miss the bound.
Values may be sent and summed in bfloat16 or wider, within the bound.
A program may use at most 128 MiB of HBM per device.

v0:
```python
import jax
import jax.numpy as jnp
from jax import lax
from jax.sharding import PartitionSpec as P

D = 2048
LRU_BLOCK = 64
CONV_TAPS = 4
lru_const = 8.0
norm_eps = 1e-06


def from_behind(value, axis, steps):
    count = lax.axis_size(axis)
    leading, last = (max(0, -steps), min(count, count - steps))
    return lax.ppermute(value, axis, [(source, source + steps) for source in range(leading, last)])


def rms_scale(values, gain):
    multiplier = lax.rsqrt(jnp.mean(values * values, axis=-1, keepdims=True) + norm_eps)
    return values * multiplier * gain


def merge_state(earlier, later):
    return (earlier[0] * later[0], later[0] * earlier[1] + later[1])


def block_length(length, span):
    shards = max(length // span, 1)
    group_size = 1
    for trial_size in range(1, shards + 1):
        if shards % trial_size == 0 and trial_size * span <= 1024:
            group_size = trial_size
    sub_size = group_size * span
    if length % sub_size:
        sub_size = length
    return sub_size


def body(
    inputs,
    norm_gain,
    query_weight,
    key_weight,
    value_weight,
    query_gain,
    key_gain,
    forget_cache,
    rec_in_weight,
    rec_gate_weight,
    conv_weight,
    decay_gate_weight,
    input_gate_weight,
    decay_param,
    decay_extra,
    attn_out_gain,
    rec_out_gain,
    out_att_weight,
    out_rec_weight,
):
    seq_count, seq_span, model_width = inputs.shape
    row_count = seq_count * seq_span
    head_dim = query_gain.shape[0]
    att_local = query_weight.shape[1] // head_dim
    kv_local = key_weight.shape[1] // head_dim
    head_group = att_local // kv_local
    channels = rec_in_weight.shape[1]
    normed = rms_scale(
        inputs.reshape(row_count, model_width).astype(jnp.float32), norm_gain
    ).astype(jnp.bfloat16)
    normed_cols = normed.T
    row_contract = (((0,), (0,)), ((), ()))
    kv_cols = key_weight.shape[1]
    pieces = (
        lax.all_gather(query_weight, "sp", axis=0, tiled=True),
        lax.all_gather(key_weight, "sp", axis=0, tiled=True),
        lax.all_gather(value_weight, "sp", axis=0, tiled=True),
        lax.all_gather(rec_in_weight, "sp", axis=0, tiled=True),
        lax.all_gather(rec_gate_weight, "sp", axis=0, tiled=True),
    )
    query_proj, key_proj, value_sum, rec_in_sum, gate_proj = tuple(
        (
            lax.dot_general(
                normed_cols, weight_part, row_contract, preferred_element_type=jnp.float32
            )
            for weight_part in pieces
        )
    )
    queries = rms_scale(query_proj.reshape(row_count, att_local, head_dim), query_gain).astype(
        jnp.bfloat16
    )
    queries = queries.reshape(seq_count, seq_span, kv_local, head_group, head_dim).transpose(
        0, 2, 3, 1, 4
    )
    queries = queries.reshape(seq_count, kv_local, head_group * seq_span, head_dim)
    key_heads = rms_scale(key_proj.reshape(row_count, kv_local, head_dim), key_gain).astype(
        jnp.bfloat16
    )
    key_heads = key_heads.reshape(seq_count, seq_span, kv_cols)
    value_heads = value_sum.astype(jnp.bfloat16).reshape(seq_count, seq_span, kv_cols)
    key_value = jnp.concatenate([key_heads, value_heads], axis=2)
    my_first = lax.axis_index("sp") * seq_span
    own_gates = lax.dynamic_slice_in_dim(forget_cache, my_first, seq_span, 2)
    own_gates = own_gates.reshape(seq_count, kv_local, head_group, seq_span, 1)
    query_pos = my_first + jnp.tile(jnp.arange(seq_span, dtype=jnp.int32), head_group)
    scaling = head_dim ** (-0.5)
    start_state = (
        jnp.full((seq_count, kv_local, head_group * seq_span), -jnp.inf, jnp.float32),
        jnp.zeros((seq_count, kv_local, head_group * seq_span), jnp.float32),
        jnp.zeros((seq_count, kv_local, head_group * seq_span, head_dim), jnp.float32),
    )
    shard_part = lax.all_gather(key_value, "sp", axis=1, tiled=True)
    offset = jnp.int32(0)
    length = shard_part.shape[1]
    sub_size = block_length(length, seq_span)

    def one_step(block_index, carried_state):
        key_first = offset + block_index * sub_size

        def work(carried):
            top_score, totals, accum = carried
            block_rows = lax.dynamic_slice_in_dim(shard_part, block_index * sub_size, sub_size, 1)
            key_block = block_rows[:, :, :kv_cols].reshape(seq_count, sub_size, kv_local, head_dim)
            value_block = block_rows[:, :, kv_cols:].reshape(
                seq_count, sub_size, kv_local, head_dim
            )
            key_gates = lax.dynamic_slice_in_dim(forget_cache, key_first, sub_size, 2)
            key_gates = key_gates.reshape(seq_count, kv_local, head_group, 1, sub_size)
            scores = (
                jnp.einsum(
                    "bhqd,bkhd->bhqk", queries, key_block, preferred_element_type=jnp.float32
                )
                * scaling
            )
            scores = (
                scores.reshape(seq_count, kv_local, head_group, seq_span, sub_size)
                + own_gates
                - key_gates
            )
            scores = scores.reshape(seq_count, kv_local, head_group * seq_span, sub_size)
            visible = (
                query_pos[:, None] >= (key_first + jnp.arange(sub_size, dtype=jnp.int32))[None, :]
            )
            scores = jnp.where(visible, scores, -jnp.inf)
            new_top = jnp.maximum(top_score, jnp.max(scores, axis=-1))
            safe_top = jnp.where(jnp.isfinite(new_top), new_top, 0.0)
            weights = jnp.exp(scores - safe_top[..., None])
            fading = jnp.exp(top_score - safe_top)
            totals = totals * fading + jnp.sum(weights, axis=-1)
            accum = accum * fading[..., None] + jnp.einsum(
                "bhqk,bkhd->bhqd",
                weights.astype(jnp.bfloat16),
                value_block,
                preferred_element_type=jnp.float32,
            )
            return (new_top, totals, accum)

        return lax.cond(
            key_first < my_first + seq_span, work, lambda carried: carried, carried_state
        )

    top_score, totals, accum = lax.fori_loop(0, length // sub_size, one_step, start_state)
    attended = (accum / totals[..., None]).reshape(
        seq_count, kv_local, head_group, seq_span, head_dim
    )
    attended = attended.transpose(0, 3, 1, 2, 4).reshape(row_count, att_local, head_dim)
    att_normed = rms_scale(attended, attn_out_gain.reshape(att_local, head_dim)).astype(
        jnp.bfloat16
    )
    att_normed = att_normed.reshape(row_count, att_local * head_dim)
    rec_in = rec_in_sum.astype(jnp.bfloat16).reshape(seq_count, seq_span, channels)
    before = from_behind(rec_in[:, seq_span - (CONV_TAPS - 1) :, :], "sp", 1)
    extended = jnp.concatenate([before, rec_in], axis=1)
    conv = jnp.zeros((seq_count, seq_span, channels), jnp.float32)
    for tap in range(CONV_TAPS):
        conv = conv + extended[:, tap : tap + seq_span].astype(jnp.float32) * conv_weight[
            tap
        ].astype(jnp.float32)
    conv = conv.astype(jnp.bfloat16)
    blocks_local = decay_gate_weight.shape[0]
    grouped = conv.reshape(seq_count, seq_span, blocks_local, LRU_BLOCK)
    gate_decay = jnp.einsum(
        "bsnd,nde->bsne", grouped, decay_gate_weight, preferred_element_type=jnp.float32
    ).reshape(seq_count, seq_span, channels)
    gate_input = jnp.einsum(
        "bsnd,nde->bsne", grouped, input_gate_weight, preferred_element_type=jnp.float32
    ).reshape(seq_count, seq_span, channels)
    log_decay = (
        -lru_const * jax.nn.sigmoid(gate_decay) * jax.nn.softplus(-decay_param) + decay_extra
    )
    drive = (
        jnp.sqrt(-jnp.expm1(2.0 * log_decay))
        * jax.nn.sigmoid(gate_input)
        * conv.astype(jnp.float32)
    )
    cum_decay, local_state = lax.associative_scan(merge_state, (jnp.exp(log_decay), drive), axis=1)
    every_decay, every_state = (
        lax.all_gather(cum_decay[:, seq_span - 1][None], "sp", axis=0, tiled=True),
        lax.all_gather(local_state[:, seq_span - 1][None], "sp", axis=0, tiled=True),
    )
    prefix_decay, prefix_state = lax.associative_scan(
        merge_state, (every_decay, every_state), axis=0
    )
    position = lax.axis_index("sp")
    earlier_state = lax.dynamic_index_in_dim(
        prefix_state, jnp.maximum(position - 1, 0), 0, keepdims=False
    )
    entering = jnp.where(position > 0, earlier_state, 0.0)
    state = local_state + cum_decay * entering[:, None, :]
    gated = state * jax.nn.gelu(gate_proj.reshape(seq_count, seq_span, channels))
    rec_normed = rms_scale(
        gated.reshape(row_count, blocks_local, LRU_BLOCK),
        rec_out_gain.reshape(blocks_local, LRU_BLOCK),
    ).astype(jnp.bfloat16)
    rec_normed = rec_normed.reshape(row_count, channels)
    out_cols = D // lax.axis_size("tp")
    pieces = row_count * lax.axis_size("tp") // row_count
    terms = jnp.dot(att_normed, out_att_weight, preferred_element_type=jnp.float32) + jnp.dot(
        rec_normed, out_rec_weight, preferred_element_type=jnp.float32
    )
    mixed_cols = lax.psum_scatter(
        terms.reshape(row_count, pieces, out_cols)
        .transpose(1, 0, 2)
        .reshape(pieces * row_count, out_cols)
        .astype(jnp.bfloat16),
        "tp",
        scatter_dimension=0,
        tiled=True,
    )
    return mixed_cols.reshape(seq_count, seq_span, out_cols)


def solution(mesh):
    return jax.shard_map(
        body,
        mesh=mesh,
        in_specs=(
            P(None, "sp", None),
            P(),
            P("sp", "tp"),
            P("sp", "tp"),
            P("sp", "tp"),
            P(),
            P(),
            P(None, "tp", None),
            P("sp", "tp"),
            P("sp", "tp"),
            P(None, "tp"),
            P("tp", None, None),
            P("tp", None, None),
            P("tp"),
            P(None, "sp", "tp"),
            P("tp"),
            P("tp"),
            P("tp", None),
            P("tp", None),
        ),
        out_specs=P(None, "sp", "tp"),
        check_vma=False,
    )
```

profile of v0, /device:TPU:0, one launch (start us, length us, event | category | flops | bytes accessed | tf_op | source)
XLA Modules:
  0.0 263.9 jit_solution(10849590766930557368)
XLA Ops:
  9.5 1.5 multiply_reduce_fusion
  11.0 1.4 slice_convert_fusion.3
  12.4 33.4 %all_gather.25 = bf16[2048,64]{0,1:T(8,128)(2,1)S(1)} all-gather(bf16[256,64]{0,1:T(8,128)(2,1)} %param.24), channel_id=1, replica_groups=mesh['sp'=8,'tp'=4] {'sp'}, dimensions={0}, use_global_device_ids=true | all-gather | bytes 294912 | tf_op jit(solution)/shard_map/all_gather | solution.py:76
  45.8 31.4 %all_gather.26 = bf16[2048,64]{0,1:T(8,128)(2,1)S(1)} all-gather(bf16[256,64]{0,1:T(8,128)(2,1)} %param.25), channel_id=1, replica_groups=mesh['sp'=8,'tp'=4] {'sp'}, dimensions={0}, use_global_device_ids=true | all-gather | bytes 294912 | tf_op jit(solution)/shard_map/all_gather | solution.py:77
  77.2 1.0 fusion.14
  79.3 29.7 %all_gather.27 = bf16[2,1024,128]{1,2,0:T(8,128)(2,1)} all-gather(bf16[2,128,128]{1,2,0:T(8,128)(2,1)S(1)} %pad_maximum_fusion.3), channel_id=1, replica_groups=mesh['sp'=8,'tp'=4] {'sp'}, dimensions={1}, use_global_device_ids=true | all-gather | bytes 589824 | tf_op jit(solution)/shard_map/all_gather | solution.py:112
  108.9 1.3 multiply_convert_fusion
  110.3 2.4 copy.49
  112.6 1.7 multiply_reduce_fusion.1
  114.6 6.3 %conditional.1 = ((f32[2,1,512]{2,0,1:T(2,128)S(1)}, f32[2,1,512,64]{2,3,0,1:T(8,128)S(1)})) conditional(s32[]{:T(128)} %convert_element_type.124, (f32[2,1,512]{2,0,1:T(2,128)S(1)}, f32[2,1,512,64]{2,3,0,1:T(8,128)S(1)}) %tuple.30, (s32[]{:T(128)}, s32[4,128]{1,0:T(4,128)S(1)}, bf16[2,1,4,128,64]{3,2,4,0,1:T(4,128)(2,1)S(1)}, ...), branch_computations={%region_3.4_spmd, %region_4.7_spmd} | conditional | flops 281680384 | bytes 17967226 | solution.py:158
  114.7 0.8 dynamic-slice_bitcast_fusion
  115.9 2.4 fusion.3
  118.4 1.8 fusion.1
  120.2 0.8 fusion.4
  121.5 1.7 convolution_convert_fusion
  123.3 3.3 %collective-permute-start = (bf16[2,3,256]{2,1,0:T(4,128)(2,1)S(1)}, bf16[2,3,256]{2,1,0:T(4,128)(2,1)S(1)}, u32[]{:S(2)}, u32[]{:S(2)}) collective-permute-start(bf16[2,3,256]{2,1,0:T(4,128)(2,1)S(1)} %slice.399), channel_id=1, source_target_pairs={{0,4},{4,8},{8,12},{12,16},{16,20},{20,24},{24,28},{1,5},{5,9},{9,... | collective-permute-start | bytes 9224 | tf_op jit(solution)/shard_map/ppermute | solution.py:16
  129.1 0.8 copy.62
  129.9 1.2 fusion.22
  131.1 0.8 copy.58
  132.0 2.0 convert_multiply_fusion
  134.7 1.6 slice.363
  136.4 1.0 slice.317
  137.3 1.6 slice.316
  141.6 1.1 multiply_add_fusion.1
  147.7 0.8 fusion.53
  149.2 0.8 pad.128
  151.9 0.9 pad_maximum_fusion.4
  152.8 2.1 pad.116
  154.9 0.8 pad.130
  155.7 1.6 add.383
  157.3 1.7 fusion.45
  159.0 1.5 pad.117
  160.5 2.3 pad.118
  162.8 0.7 slice_add_fusion.4
  163.6 26.3 %all-gather = f32[16,1,256]{2,1,0:T(1,128)S(1)} all-gather(f32[2,1,256]{2,1,0:T(1,128)S(1)} %slice_add_fusion.4), channel_id=2, replica_groups=mesh['sp'=8,'tp'=4] {'sp'}, dimensions={0}, use_global_device_ids=true | all-gather | bytes 18432 | tf_op jit(solution)/shard_map/all_gather | solution.py:199
  190.4 1.6 pad_maximum_fusion.2
  192.0 0.9 pad.131
  193.6 0.7 reshape.378
  194.3 1.2 copy.63
  195.6 1.4 pad.132
  197.7 26.1 %all-gather.1 = f32[16,1,256]{2,1,0:T(1,128)S(1)} all-gather(f32[2,1,256]{2,1,0:T(1,128)S(1)} %slice_add_fusion.3), channel_id=3, replica_groups=mesh['sp'=8,'tp'=4] {'sp'}, dimensions={0}, use_global_device_ids=true | all-gather | bytes 18432 | tf_op jit(solution)/shard_map/all_gather | solution.py:198
  224.9 3.0 %fusion.73 = (f32[2,128,256]{2,1,0:T(8,128)}, f32[2,128,256]{2,1,0:T(8,128)}) fusion(bf16[2,128,2048]{2,1,0:T(8,128)(2,1)} %multiply_convert_fusion, bf16[2048,256]{1,0:T(8,128)(2,1)} %all-gather.10.cloned.1.call-done, f32[2,256]{1,0:T(2,128)S(1)} %fusion.65, f32[2,128,256]{2,1,0:T(8,128)S(1)} %pad.131, f32[2,128,256]{2,1,0:T(8,128)} %pad.132, ...), kind=kOutput, calls=%fused_computation.170 | convolution fusion | flops 269352960 | bytes 3672064 | tf_op jit(solution)/shard_map/dot_general | solution.py:83
  227.9 1.8 copy.64
  229.7 1.2 mul.431
  230.9 1.1 copy.65
  232.1 1.7 fusion.12
  233.8 1.1 copy.94
  234.9 22.5 %reduce-scatter.2.cloned.1.call-done = bf16[256,512]{1,0:T(8,128)(2,1)} async-done(((bf16[1024,512]{1,0:T(8,128)(2,1)}), bf16[256,512]{1,0:T(8,128)(2,1)}) %reduce-scatter.2.cloned.1.call-update) | async-done | bytes 262160 | tf_op jit(solution)/shard_map/reduce_scatter | solution.py:221
  (192 shorter events, 21.6 us)
Async XLA Ops:
  6.5 120.2 %copy-start = (bf16[256,2048]{1,0:T(8,128)(2,1)S(1)}, bf16[256,2048]{1,0:T(8,128)(2,1)}, u32[]{:S(2)}) copy-start(bf16[256,2048]{1,0:T(8,128)(2,1)} %param.38) | copy-start | bytes 3145732
  6.5 70.7 %copy-start.1 = (bf16[2,128,2048]{2,1,0:T(8,128)(2,1)S(1)}, bf16[2,128,2048]{2,1,0:T(8,128)(2,1)}, u32[]{:S(2)}) copy-start(bf16[2,128,2048]{2,1,0:T(8,128)(2,1)} %param.21) | copy-start | bytes 3145732
  6.5 103.7 %all-gather.6.cloned.1.call-start = ((), (), s32[]{:S(2)}) async-start(), calls=%async_computation.1 | async-start | bytes 1179648 | tf_op jit(solution)/shard_map/all_gather | solution.py:75
  7.3 114.3 %all-gather.8.cloned.1.call-start = ((), (), s32[]{:S(2)}) async-start(), calls=%async_computation.2 | async-start | bytes 1179648 | tf_op jit(solution)/shard_map/all_gather | solution.py:78
  8.0 216.8 %all-gather.10.cloned.1.call-start = ((), (), s32[]{:S(2)}) async-start(), calls=%async_computation.3 | async-start | bytes 1179648 | tf_op jit(solution)/shard_map/all_gather | solution.py:79
  8.7 248.6 %reduce-scatter.2.cloned.1.call-start = ((), (), s32[]{:S(2)}) async-start(), calls=%async_computation.4 | async-start | bytes 1310720 | tf_op jit(solution)/shard_map/reduce_scatter | solution.py:221
  77.2 2.0 copy-start.15
  78.2 30.7 %copy-start.8 = (f32[2048]{0:T(1024)S(1)}, f32[2048]{0:T(1024)}, u32[]{:S(2)}) copy-start(f32[2048]{0:T(1024)} %param.22) | copy-start | bytes 24580
  110.2 2.4 copy-start.2
  112.6 1.7 copy-start.16
  115.9 2.5 copy-start.6
  118.3 1.8 copy-start.3
  121.0 5.6 %copy-start.13 = (f32[256]{0:T(256)S(1)}, f32[256]{0:T(256)}, u32[]{:S(2)}) copy-start(f32[256]{0:T(256)} %param.36) | copy-start | bytes 3076
  123.2 4.6 %copy-start.9 = (f32[1,256]{1,0:T(1,128)S(1)}, f32[1,256]{1,0:T(1,128)}, u32[]{:S(2)}) copy-start(f32[1,256]{1,0:T(1,128)} %get-tuple-element.199) | copy-start | bytes 3076
  123.2 4.6 %copy-start.10 = (f32[1,256]{1,0:T(1,128)S(1)}, f32[1,256]{1,0:T(1,128)}, u32[]{:S(2)}) copy-start(f32[1,256]{1,0:T(1,128)} %get-tuple-element.200) | copy-start | bytes 3076
  123.2 4.6 %copy-start.11 = (f32[1,256]{1,0:T(1,128)S(1)}, f32[1,256]{1,0:T(1,128)}, u32[]{:S(2)}) copy-start(f32[1,256]{1,0:T(1,128)} %get-tuple-element.201) | copy-start | bytes 3076
  123.2 4.6 %copy-start.12 = (f32[1,256]{1,0:T(1,128)S(1)}, f32[1,256]{1,0:T(1,128)}, u32[]{:S(2)}) copy-start(f32[1,256]{1,0:T(1,128)} %get-tuple-element.202) | copy-start | bytes 3076
  123.3 4.6 %collective-permute-start = (bf16[2,3,256]{2,1,0:T(4,128)(2,1)S(1)}, bf16[2,3,256]{2,1,0:T(4,128)(2,1)S(1)}, u32[]{:S(2)}, u32[]{:S(2)}) collective-permute-start(bf16[2,3,256]{2,1,0:T(4,128)(2,1)S(1)} %slice.399), channel_id=1, source_target_pairs={{0,4},{4,8},{8,12},{12,16},{16,20},{20,24},{24,28},{1,5},{5,9},{9,... | collective-permute-start | bytes 9224 | tf_op jit(solution)/shard_map/ppermute | solution.py:16
  126.6 2.2 copy-start.17
  128.1 0.7 copy-start.7
  144.1 7.1 %copy-start.4 = (f32[2,31,256]{2,1,0:T(8,128)S(1)}, f32[2,31,256]{2,1,0:T(8,128)}, u32[]{:S(2)}) copy-start(f32[2,31,256]{2,1,0:T(8,128)} %slice.361) | copy-start | bytes 190468
  144.2 7.1 %copy-start.5 = (f32[2,31,256]{2,1,0:T(8,128)S(1)}, f32[2,31,256]{2,1,0:T(8,128)}, u32[]{:S(2)}) copy-start(f32[2,31,256]{2,1,0:T(8,128)} %slice.320) | copy-start | bytes 190468
  224.8 7.1 %copy-start.14 = (f32[256]{0:T(256)S(1)}, f32[256]{0:T(256)}, u32[]{:S(2)}) copy-start(f32[256]{0:T(256)} %param.37) | copy-start | bytes 3076
Sparse Core Ops, SparseCore 0:
  9.5 44.2 all-gather.5
  55.9 41.5 all-gather.7
  99.6 38.9 all-gather.9
  235.0 22.3 reduce-scatter.1
where the time goes:
time: 265 us; the launch traced here: 264 us
  blocking collectives  147 us (55%)
  local copies, waits for them, and re-layouts  35.4 us (13%)
  waiting for transfers between devices  25.4 us (10%)
  other arithmetic  24.8 us (9%)
  matrix products  14.1 us (5%)
  between operations  13.9 us (5%)
  starting transfers between devices  3.38 us (1%)
    all_gather x1, blocking collectives, body(): lax.all_gather(key_weight, 'sp', axis=0, tiled=True)  33.4 us
    all_gather x1, blocking collectives, body(): lax.all_gather(value_weight, 'sp', axis=0, tiled=True)  31.4 us
    all_gather x1, blocking collectives, body(): shard_part = lax.all_gather(key_value, 'sp', axis=1, tiled=True)  29.7 us
    all_gather x1, blocking collectives, body(): lax.all_gather(local_state[:, seq_span - 1][None], 'sp', axis=0, tiled=True)  26.3 us
    all_gather x1, blocking collectives, body(): lax.all_gather(cum_decay[:, seq_span - 1][None], 'sp', axis=0, tiled=True)  26.1 us
    reduce_scatter x1, waiting for transfers between devices, body(): lax.psum_scatter(terms.reshape(row_count, pieces, out_cols).transpose(1,...  22.5 us
    slice x44, local copies, waits for them, and re-layouts, body(): lax.associative_scan(merge_state, (jnp.exp(log_decay), drive), axis=1)  11.2 us
    pad x24, local copies, waits for them, and re-layouts, body(): lax.associative_scan(merge_state, (jnp.exp(log_decay), drive), axis=1)  10.2 us
  transfers between devices with their start and end apart: 5, of which 2 were waited for; matrix products, arithmetic and copies ran while one was open for 24% of the time, Pallas kernels for 0%

commit v1 on v0

--- a/solution.py
+++ b/solution.py
@@ -8,6 +8,27 @@
 CONV_TAPS = 4
 lru_const = 8.0
 norm_eps = 1e-06
+
+
+def ring_gather(x, axis, dim):
+    length, index, rows = (lax.axis_size(axis), lax.axis_index(axis), x.shape[dim])
+    right = [(i, (i + 1) % length) for i in range(length)]
+    left = [(i, (i - 1) % length) for i in range(length)]
+    out = jnp.zeros((*x.shape[:dim], length * rows, *x.shape[dim + 1 :]), x.dtype)
+    out = lax.dynamic_update_slice_in_dim(out, x, index * rows, axis=dim)
+    from_left = from_right = x
+    halfway = length // 2
+    for step in range(1, halfway + 1):
+        from_left = lax.ppermute(from_left, axis, right)
+        out = lax.dynamic_update_slice_in_dim(
+            out, from_left, (index - step) % length * rows, axis=dim
+        )
+        if step < length - halfway:
+            from_right = lax.ppermute(from_right, axis, left)
+            out = lax.dynamic_update_slice_in_dim(
+                out, from_right, (index + step) % length * rows, axis=dim
+            )
+    return out
 
 
 def from_behind(value, axis, steps):
@@ -109,7 +130,7 @@
         jnp.zeros((seq_count, kv_local, head_group * seq_span), jnp.float32),
         jnp.zeros((seq_count, kv_local, head_group * seq_span, head_dim), jnp.float32),
     )
-    shard_part = lax.all_gather(key_value, "sp", axis=1, tiled=True)
+    shard_part = ring_gather(key_value, "sp", 1)
     offset = jnp.int32(0)
     length = shard_part.shape[1]
     sub_size = block_length(length, seq_span)

time: 265 us -> 328 us (1.24)
  local copies, waits for them, and re-layouts: 35.4 us -> 90.6 us
  blocking collectives: 147 us -> 117 us
  other arithmetic: 24.8 us -> 38.4 us
  starting transfers between devices: 3.38 us -> 16.3 us
  waiting for transfers between devices: 25.4 us -> 32.6 us
    slice x44, local copies, waits for them, and re-layouts: 11.2 us -> 51.4 us  [body(): lax.associative_scan(merge_state, (jnp.exp(log_decay), drive), axis=1)]
    all_gather x1 -> x0, blocking collectives: 29.7 us -> none  [body(): shard_part = lax.all_gather(key_value, 'sp', axis=1, tiled=True)]
    ppermute x0 -> x7, starting transfers between devices: none -> 14.6 us  [the longest x3 12.3 us: ring_gather(): from_right = lax.ppermute(from_right, axis, left)]
    sub x0 -> x2, local copies, waits for them, and re-layouts: none -> 9.52 us  [work(): scores.reshape(seq_count, kv_local, head_group, seq_span, sub_size)]
    add x13, other arithmetic: 4.34 us -> 13.8 us  [merge_state(): return (earlier[0] * later[0], later[0] * earlier[1] + later[1])]
    ppermute x0 -> x7, waiting for transfers between devices: none -> 8.25 us  [the longest x4 7.34 us: ring_gather(): from_left = lax.ppermute(from_left, axis, right)]
    dynamic_update_slice x0 -> x8, local copies, waits for them, and re-layouts: none -> 5.52 us  [the longest x4 2.61 us: ring_gather(): lax.dynamic_update_slice_in_dim(out, from_left, (index - step) % length *...]
    concatenate x11, other arithmetic: 3.16 us -> 7.84 us  [body(): lax.associative_scan(merge_state, (jnp.exp(log_decay), drive), axis=1)]
  transfers between devices with their start and end apart: 5 -> 12, of which waited for: 2 -> 7; matrix products, arithmetic and copies ran while one was open for 24% -> 41% of each run, Pallas kernels for 0% -> 0%
where the time goes in v1:
time: 328 us; the launch traced here: 324 us
  blocking collectives  117 us (36%)
  local copies, waits for them, and re-layouts  90.6 us (28%)
  other arithmetic  38.4 us (12%)
  waiting for transfers between devices  32.6 us (10%)
  starting transfers between devices  16.3 us (5%)
  matrix products  15.1 us (5%)
  between operations  13.9 us (4%)
    slice x44, local copies, waits for them, and re-layouts, body(): lax.associative_scan(merge_state, (jnp.exp(log_decay), drive), axis=1)  51.4 us
    all_gather x1, blocking collectives, body(): lax.all_gather(key_weight, 'sp', axis=0, tiled=True)  33.1 us
    all_gather x1, blocking collectives, body(): lax.all_gather(value_weight, 'sp', axis=0, tiled=True)  31.4 us
    all_gather x1, blocking collectives, body(): lax.all_gather(cum_decay[:, seq_span - 1][None], 'sp', axis=0, tiled=True)  26.1 us
    all_gather x1, blocking collectives, body(): lax.all_gather(local_state[:, seq_span - 1][None], 'sp', axis=0, tiled=True)  26.1 us
    reduce_scatter x1, waiting for transfers between devices, body(): lax.psum_scatter(terms.reshape(row_count, pieces, out_cols).transpose(1,...  22.9 us
    add x13, other arithmetic, merge_state(): return (earlier[0] * later[0], later[0] * earlier[1] + later[1])  13.8 us
    ppermute x3, starting transfers between devices, ring_gather(): from_right = lax.ppermute(from_right, axis, left)  12.3 us
  transfers between devices with their start and end apart: 12, of which 7 were waited for; matrix products, arithmetic and copies ran while one was open for 41% of the time, Pallas kernels for 0%

profile of v1, /device:TPU:0, one launch (start us, length us, event | category | flops | bytes accessed | tf_op | source)
XLA Modules:
  0.0 323.7 jit_solution(13435449004433587643)
XLA Ops:
  8.1 1.5 multiply_reduce_fusion
  9.6 33.1 %all_gather.21 = bf16[2048,64]{0,1:T(8,128)(2,1)S(1)} all-gather(bf16[256,64]{0,1:T(8,128)(2,1)} %param.24), channel_id=1, replica_groups=mesh['sp'=8,'tp'=4] {'sp'}, dimensions={0}, use_global_device_ids=true | all-gather | bytes 294912 | tf_op jit(solution)/shard_map/all_gather | solution.py:97
  42.7 31.4 %all_gather.22 = bf16[2048,64]{0,1:T(8,128)(2,1)S(1)} all-gather(bf16[256,64]{0,1:T(8,128)(2,1)} %param.25), channel_id=1, replica_groups=mesh['sp'=8,'tp'=4] {'sp'}, dimensions={0}, use_global_device_ids=true | all-gather | bytes 294912 | tf_op jit(solution)/shard_map/all_gather | solution.py:98
  74.1 1.5 fusion.20
  76.6 1.6 collective-permute-start
  78.3 3.1 collective-permute-start.1
  85.2 4.2 %collective-permute-start.3 = (bf16[2,128,128]{1,2,0:T(8,128)(2,1)S(1)}, bf16[2,128,128]{1,2,0:T(8,128)(2,1)}, u32[]{:S(2)}, u32[]{:S(2)}) collective-permute-start(bf16[2,128,128]{1,2,0:T(8,128)(2,1)S(1)} %collective-permute-done.1), channel_id=1, source_target_pairs={{0,28},{4,0},{8,4},{12,8},{16,12},{20,16},{24,20},{28,24},{1,29},{... | collective-permute-start | bytes 196616 | tf_op jit(solution)/shard_map/ppermute | solution.py:27
  91.5 5.0 %collective-permute-start.5 = (bf16[2,128,128]{1,2,0:T(8,128)(2,1)}, bf16[2,128,128]{1,2,0:T(8,128)(2,1)}, u32[]{:S(2)}, u32[]{:S(2)}) collective-permute-start(bf16[2,128,128]{1,2,0:T(8,128)(2,1)} %collective-permute-done.3), channel_id=1, source_target_pairs={{0,28},{4,0},{8,4},{12,8},{16,12},{20,16},{24,20},{28,24},{1,29},{... | collective-permute-start | bytes 196616 | tf_op jit(solution)/shard_map/ppermute | solution.py:27
  96.5 1.9 collective-permute-done.4
  98.5 1.5 copy.58
  100.0 1.7 multiply_reduce_fusion.1
  102.6 3.1 collective-permute-done.6
  105.7 24.2 %conditional.1 = ((f32[2,1,512]{2,0,1:T(2,128)S(1)}, f32[2,1,512,64]{2,3,0,1:T(8,128)S(1)})) conditional(s32[]{:T(128)} %convert_element_type.126, (f32[2,1,512]{2,0,1:T(2,128)S(1)}, f32[2,1,512,64]{2,3,0,1:T(8,128)S(1)}) %tuple.93, (s32[]{:T(128)}, s32[4,128]{1,0:T(4,128)S(1)}, bf16[2,128,128]{1,2,0:T(8,128)(2,1)S(1)}, s32[]{:T(128)}, ...), branch_computations={%region_3.4_spmd, %region_4.7_spmd.clone.clone} | conditional | flops 278534784 | bytes 39890236 | solution.py:179
  114.6 3.9 %sub.101 = f32[2,4,128,1024]{2,1,3,0:T(4,128)} broadcast(f32[2,4,1024]{1,2,0:T(8,128)S(1)} %copy.81), dimensions={0,1,3} | broadcast | bytes 4227072 | tf_op jit(solution)/shard_map/while/body/eval_jaxpr/cond/branch_1_fun/sub | solution.py:157
  118.6 5.6 %sub.102 = f32[2,512,1024]{1,2,0:T(8,128)} reshape(f32[2,4,128,1024]{2,1,3,0:T(4,128)} %sub.101) | data formatting | bytes 8388608 | tf_op jit(solution)/shard_map/while/body/eval_jaxpr/cond/branch_1_fun/sub | solution.py:157
  125.1 3.4 %fusion.75 = (f32[2,512]{1,0:T(2,128)S(1)}, f32[2,512,1024]{1,2,0:T(8,128)S(1)}) fusion(f32[2,512,1024]{1,2,0:T(8,128)} %sub.102, f32[2,512]{1,0:T(2,128)S(1)} %bitcast.180, bf16[2,512,64]{1,2,0:T(8,128)(2,1)S(1)} %reshape.403, bf16[2,1024,128]{1,2,0:T(8,128)(2,1)S(1)} %copy-done.4, pred[512,1024]{0,1:T(8,128)(4,1)S(1)} %copy-done.2), kind=kOutput, calls=%fused_computation.172 | convolution fusion | flops 139459584 | bytes 9314304 | tf_op jit(solution)/shard_map/while/body/eval_jaxpr/cond/branch_1_fun/bhqd,bkhd->bhqk/dot_general | solution.py:151
  130.6 1.7 convolution_convert_fusion
  132.3 1.5 collective-permute-start.7
  139.2 2.0 convert_multiply_fusion
  141.2 1.6 slice.320
  142.8 1.6 slice.321
  145.8 1.8 multiply_add_fusion.1
  147.6 1.5 slice.326
  149.1 1.5 slice.327
  151.9 1.6 multiply_add_fusion.2
  153.5 1.5 slice.332
  155.0 1.4 slice.333
  156.4 1.4 slice.331
  157.9 1.4 slice.335
  159.3 1.4 multiply_add_fusion.3
  189.2 1.4 slice.330
  190.6 1.5 slice.363
  195.3 1.5 slice.365
  199.4 1.6 slice.367
  212.5 1.5 fusion.55
  215.6 1.5 pad_maximum_fusion.4
  217.1 2.1 pad.129
  219.8 1.6 add.516
  221.4 1.7 fusion.51
  223.2 2.3 pad.118
  226.4 1.4 pad.131
  227.8 2.3 pad.132
  231.6 26.1 %all-gather = f32[16,1,256]{2,1,0:T(1,128)S(1)} all-gather(f32[2,1,256]{2,1,0:T(1,128)S(1)} %slice_add_fusion.4), channel_id=2, replica_groups=mesh['sp'=8,'tp'=4] {'sp'}, dimensions={0}, use_global_device_ids=true | all-gather | bytes 18432 | tf_op jit(solution)/shard_map/all_gather | solution.py:220
  257.7 26.1 %all-gather.1 = f32[16,1,256]{2,1,0:T(1,128)S(1)} all-gather(f32[2,1,256]{2,1,0:T(1,128)S(1)} %slice_add_fusion.3), channel_id=3, replica_groups=mesh['sp'=8,'tp'=4] {'sp'}, dimensions={0}, use_global_device_ids=true | all-gather | bytes 18432 | tf_op jit(solution)/shard_map/all_gather | solution.py:219
  284.3 3.0 fusion.80
  287.3 1.8 copy.71
  291.5 1.7 fusion.18
  294.3 22.9 %reduce-scatter.2.cloned.1.call-done = bf16[256,512]{1,0:T(8,128)(2,1)} async-done(((bf16[1024,512]{1,0:T(8,128)(2,1)}), bf16[256,512]{1,0:T(8,128)(2,1)}) %reduce-scatter.2.cloned.1.call-update) | async-done | bytes 262160 | tf_op jit(solution)/shard_map/reduce_scatter | solution.py:242
  (222 shorter events, 82.9 us)
Async XLA Ops:
  6.5 128.0 %copy-start = (bf16[256,2048]{1,0:T(8,128)(2,1)S(1)}, bf16[256,2048]{1,0:T(8,128)(2,1)}, u32[]{:S(2)}) copy-start(bf16[256,2048]{1,0:T(8,128)(2,1)} %param.38) | copy-start | bytes 3145732
  6.5 75.0 %copy-start.1 = (bf16[2,128,2048]{2,1,0:T(8,128)(2,1)S(1)}, bf16[2,128,2048]{2,1,0:T(8,128)(2,1)}, u32[]{:S(2)}) copy-start(bf16[2,128,2048]{2,1,0:T(8,128)(2,1)} %param.21) | copy-start | bytes 3145732
  6.5 75.0 %copy-start.8 = (f32[2048]{0:T(1024)S(1)}, f32[2048]{0:T(1024)}, u32[]{:S(2)}) copy-start(f32[2048]{0:T(1024)} %param.22) | copy-start | bytes 24580
  6.5 70.0 %copy-start.18 = (f32[64]{0:T(128)S(1)}, f32[64]{0:T(128)}, u32[]{:S(2)}) copy-start(f32[64]{0:T(128)} %param.27) | copy-start | bytes 772
  6.5 91.9 %all-gather.6.cloned.1.call-start = ((), (), s32[]{:S(2)}) async-start(), calls=%async_computation.1 | async-start | bytes 1179648 | tf_op jit(solution)/shard_map/all_gather | solution.py:96
  7.3 123.3 %all-gather.8.cloned.1.call-start = ((), (), s32[]{:S(2)}) async-start(), calls=%async_computation.2 | async-start | bytes 1179648 | tf_op jit(solution)/shard_map/all_gather | solution.py:99
  8.0 76.4 %copy-start.11 = (bf16[4,256]{1,0:T(4,128)(2,1)S(1)}, bf16[4,256]{1,0:T(4,128)(2,1)}, u32[]{:S(2)}) copy-start(bf16[4,256]{1,0:T(4,128)(2,1)} %param.31) | copy-start | bytes 6148
  8.0 82.7 %copy-start.17 = (f32[256]{0:T(256)S(1)}, f32[256]{0:T(256)}, u32[]{:S(2)}) copy-start(f32[256]{0:T(256)} %param.34) | copy-start | bytes 3076
  8.0 276.2 %all-gather.10.cloned.1.call-start = ((), (), s32[]{:S(2)}) async-start(), calls=%async_computation.3 | async-start | bytes 1179648 | tf_op jit(solution)/shard_map/all_gather | solution.py:100
  76.5 25.2 %copy-start.19 = (f32[64]{0:T(128)S(1)}, f32[64]{0:T(128)}, u32[]{:S(2)}) copy-start(f32[64]{0:T(128)} %param.26) | copy-start | bytes 772
  76.6 7.0 %collective-permute-start = (bf16[2,128,128]{1,2,0:T(8,128)(2,1)S(1)}, bf16[2,128,128]{1,2,0:T(8,128)(2,1)S(1)}, u32[]{:S(2)}, u32[]{:S(2)}) collective-permute-start(bf16[2,128,128]{1,2,0:T(8,128)(2,1)S(1)} %bitcast_dynamic-update-slice_fusion), channel_id=1, source_target_pairs={{0,4},{4,8},{8,12},{12,16},{16,20},{20,24},{24,28},{28,0},{1,5},{5... | collective-permute-start | bytes 196616 | tf_op jit(solution)/shard_map/ppermute | solution.py:22
  78.3 6.9 %collective-permute-start.1 = (bf16[2,128,128]{1,2,0:T(8,128)(2,1)S(1)}, bf16[2,128,128]{1,2,0:T(8,128)(2,1)S(1)}, u32[]{:S(2)}, u32[]{:S(2)}) collective-permute-start(bf16[2,128,128]{1,2,0:T(8,128)(2,1)S(1)} %bitcast_dynamic-update-slice_fusion), channel_id=1, source_target_pairs={{0,28},{4,0},{8,4},{12,8},{16,12},{20,16},{24,20},{28,24},{1,29},{... | collective-permute-start | bytes 196616 | tf_op jit(solution)/shard_map/ppermute | solution.py:27
  81.4 235.8 %reduce-scatter.2.cloned.1.call-start = ((), (), s32[]{:S(2)}) async-start(), calls=%async_computation.4 | async-start | bytes 1310720 | tf_op jit(solution)/shard_map/reduce_scatter | solution.py:242
  83.7 7.1 %collective-permute-start.2 = (bf16[2,128,128]{1,2,0:T(8,128)(2,1)S(1)}, bf16[2,128,128]{1,2,0:T(8,128)(2,1)S(1)}, u32[]{:S(2)}, u32[]{:S(2)}) collective-permute-start(bf16[2,128,128]{1,2,0:T(8,128)(2,1)S(1)} %collective-permute-done), channel_id=1, source_target_pairs={{0,4},{4,8},{8,12},{12,16},{16,20},{20,24},{24,28},{28,0},{1,5},{5... | collective-permute-start | bytes 196616 | tf_op jit(solution)/shard_map/ppermute | solution.py:22
  85.2 13.3 %copy-start.6 = (bf16[2,128,128]{1,2,0:T(8,128)(2,1)}, bf16[2,128,128]{1,2,0:T(8,128)(2,1)S(1)}, u32[]{:S(2)}) copy-start(bf16[2,128,128]{1,2,0:T(8,128)(2,1)S(1)} %collective-permute-done.1) | copy-start | bytes 196612
  85.2 6.3 %collective-permute-start.3 = (bf16[2,128,128]{1,2,0:T(8,128)(2,1)S(1)}, bf16[2,128,128]{1,2,0:T(8,128)(2,1)}, u32[]{:S(2)}, u32[]{:S(2)}) collective-permute-start(bf16[2,128,128]{1,2,0:T(8,128)(2,1)S(1)} %collective-permute-done.1), channel_id=1, source_target_pairs={{0,28},{4,0},{8,4},{12,8},{16,12},{20,16},{24,20},{28,24},{1,29},{... | collective-permute-start | bytes 196616 | tf_op jit(solution)/shard_map/ppermute | solution.py:27
  90.7 7.7 %copy-start.7 = (bf16[2,128,128]{1,2,0:T(8,128)(2,1)}, bf16[2,128,128]{1,2,0:T(8,128)(2,1)S(1)}, u32[]{:S(2)}) copy-start(bf16[2,128,128]{1,2,0:T(8,128)(2,1)S(1)} %collective-permute-done.2) | copy-start | bytes 196612
  90.8 7.7 %collective-permute-start.4 = (bf16[2,128,128]{1,2,0:T(8,128)(2,1)S(1)}, bf16[2,128,128]{1,2,0:T(8,128)(2,1)}, u32[]{:S(2)}, u32[]{:S(2)}) collective-permute-start(bf16[2,128,128]{1,2,0:T(8,128)(2,1)S(1)} %collective-permute-done.2), channel_id=1, source_target_pairs={{0,4},{4,8},{8,12},{12,16},{16,20},{20,24},{24,28},{28,0},{1,5},{5... | collective-permute-start | bytes 196616 | tf_op jit(solution)/shard_map/ppermute | solution.py:22
  91.5 11.1 %collective-permute-start.5 = (bf16[2,128,128]{1,2,0:T(8,128)(2,1)}, bf16[2,128,128]{1,2,0:T(8,128)(2,1)}, u32[]{:S(2)}, u32[]{:S(2)}) collective-permute-start(bf16[2,128,128]{1,2,0:T(8,128)(2,1)} %collective-permute-done.3), channel_id=1, source_target_pairs={{0,28},{4,0},{8,4},{12,8},{16,12},{20,16},{24,20},{28,24},{1,29},{... | collective-permute-start | bytes 196616 | tf_op jit(solution)/shard_map/ppermute | solution.py:27
  98.5 7.3 %collective-permute-start.6 = (bf16[2,128,128]{1,2,0:T(8,128)(2,1)}, bf16[2,128,128]{1,2,0:T(8,128)(2,1)}, u32[]{:S(2)}, u32[]{:S(2)}) collective-permute-start(bf16[2,128,128]{1,2,0:T(8,128)(2,1)} %collective-permute-done.4), channel_id=1, source_target_pairs={{0,4},{4,8},{8,12},{12,16},{16,20},{20,24},{24,28},{28,0},{1,5},{5... | collective-permute-start | bytes 196616 | tf_op jit(solution)/shard_map/ppermute | solution.py:22
  111.5 0.8 copy-start.3
  118.6 6.5 %copy-start.2 = (pred[512,1024]{0,1:T(8,128)(4,1)S(1)}, pred[512,1024]{0,1:T(8,128)(4,1)}, u32[]{:S(2)}) copy-start(pred[512,1024]{0,1:T(8,128)(4,1)} %iota_compare_fusion) | copy-start | bytes 1572868 | tf_op jit(solution)/shard_map/while/body/eval_jaxpr/cond
  118.6 6.5 %copy-start.4 = (bf16[2,1024,128]{1,2,0:T(8,128)(2,1)S(1)}, bf16[2,1024,128]{1,2,0:T(8,128)(2,1)}, u32[]{:S(2)}) copy-start(bf16[2,1024,128]{1,2,0:T(8,128)(2,1)} %copy-done.3) | copy-start | bytes 1572868 | tf_op jit(solution)/shard_map/while/body/eval_jaxpr/cond
  130.0 5.1 %copy-start.12 = (f32[1,256]{1,0:T(1,128)S(1)}, f32[1,256]{1,0:T(1,128)}, u32[]{:S(2)}) copy-start(f32[1,256]{1,0:T(1,128)} %get-tuple-element.948) | copy-start | bytes 3076
  130.0 5.1 %copy-start.13 = (f32[1,256]{1,0:T(1,128)S(1)}, f32[1,256]{1,0:T(1,128)}, u32[]{:S(2)}) copy-start(f32[1,256]{1,0:T(1,128)} %get-tuple-element.949) | copy-start | bytes 3076
  130.0 5.1 %copy-start.14 = (f32[1,256]{1,0:T(1,128)S(1)}, f32[1,256]{1,0:T(1,128)}, u32[]{:S(2)}) copy-start(f32[1,256]{1,0:T(1,128)} %get-tuple-element.950) | copy-start | bytes 3076
  130.0 5.1 %copy-start.15 = (f32[1,256]{1,0:T(1,128)S(1)}, f32[1,256]{1,0:T(1,128)}, u32[]{:S(2)}) copy-start(f32[1,256]{1,0:T(1,128)} %get-tuple-element.951) | copy-start | bytes 3076
  130.0 6.0 %copy-start.20 = (bf16[4,64,64]{2,1,0:T(8,128)(2,1)S(1)}, bf16[4,64,64]{2,1,0:T(8,128)(2,1)}, u32[]{:S(2)}) copy-start(bf16[4,64,64]{2,1,0:T(8,128)(2,1)} %param.32) | copy-start | bytes 98308
  132.3 2.8 collective-permute-start.7
  135.4 0.7 copy-start.5
  208.1 15.0 %copy-start.10 = (f32[2,1,256]{2,1,0:T(1,128)S(1)}, f32[2,1,256]{2,1,0:T(1,128)}, u32[]{:S(2)}) copy-start(f32[2,1,256]{2,1,0:T(1,128)} %slice.414) | copy-start | bytes 6148
  208.1 17.4 %copy-start.9 = (f32[2,1,256]{2,1,0:T(1,128)S(1)}, f32[2,1,256]{2,1,0:T(1,128)}, u32[]{:S(2)}) copy-start(f32[2,1,256]{2,1,0:T(1,128)} %slice.437) | copy-start | bytes 6148
  223.1 68.3 %copy-start.16 = (f32[256]{0:T(256)S(1)}, f32[256]{0:T(256)}, u32[]{:S(2)}) copy-start(f32[256]{0:T(256)} %param.37) | copy-start | bytes 3076
Sparse Core Ops, SparseCore 0:
  9.5 43.3 all-gather.5
  55.0 41.0 all-gather.7
  98.3 40.6 all-gather.9
  294.4 22.7 reduce-scatter.1
